TPU v7x, 32 devices: a whole 2x2x4 slice. The times are simulated.
32 devices in a mesh: fs: 8 (over z, y), tp: 4 (over x, core).
Axes of the slice: x: 2, y: 2, z: 4, core: 2. Of those that a mesh axis runs over, the one named last changes fastest.
Arguments:
- tokens: bfloat16 [8192, 2048], P('fs', 'tp'), may hold values from -6 to 6
- mix_gain: float32 [2048], replicated, may hold values from 0.1 to 1.9
- in_weight: float32 [2048, 1024], P('fs', 'tp'), may hold values from -0.125 to 0.125
- in_scale: float32 [1024], P('tp'), may hold values from 0.4 to 2.5
- out_weight: float32 [1024, 2048], P('tp', 'fs'), may hold values from -0.1875 to 0.1875
- out_scale: float32 [2048], P('fs'), may hold values from 0.4 to 2.5
- ffn_gain: float32 [2048], replicated, may hold values from 0.1 to 1.9
- gate_weight: float32 [2048, 6144], P('fs', 'tp'), may hold values from -0.125 to 0.125
- gate_scale: float32 [6144], P('tp'), may hold values from 0.4 to 2.5
- up_weight: float32 [2048, 6144], P('fs', 'tp'), may hold values from -0.125 to 0.125
- up_scale: float32 [6144], P('tp'), may hold values from 0.4 to 2.5
- down_weight: float32 [6144, 2048], P('tp', 'fs'), may hold values from -0.078125 to 0.078125
- down_scale: float32 [2048], P('fs'), may hold values from 0.4 to 2.5
Outputs:
- layer_out: bfloat16 [8192, 2048], P('fs', 'tp')
All inputs are finite; a program needn't handle non-finite values.
Results may differ from a plain program's by a relative error of at most 0.023.
Values may be sent and summed in bfloat16 or wider, within the bound.
A program may use at most 128 MiB of HBM per device.

v0:
```python
import jax
import jax.numpy as jnp
from jax import lax
from jax.experimental import pallas as pl
from jax.experimental.pallas import tpu as pltpu
from jax.sharding import PartitionSpec as P

GROUPS = 4
GRID_W = 64
GC = 256
WINDOWS = (2, 4, 8, 16)
EPSILON = 1e-06


IN_SPECS = (
    P("fs", "tp"),
    P(),
    P("fs", "tp"),
    P("tp"),
    P("tp", "fs"),
    P("fs"),
    P(),
    P("fs", "tp"),
    P("tp"),
    P("fs", "tp"),
    P("tp"),
    P("tp", "fs"),
    P("fs"),
)


def box_matrix(length, window):
    position = jnp.arange(length, dtype=jnp.int32)
    lower_end = jnp.clip(position - window // 2, 0, length)
    upper_end = jnp.clip(position + (window - window // 2), 0, length)
    inside = (position[None, :] >= lower_end[:, None]) & (position[None, :] < upper_end[:, None])
    return inside.astype(jnp.float32) / (upper_end - lower_end).astype(jnp.float32)[:, None]


def smooth(lattice, window):
    across = jnp.einsum(
        "jk,akc->ajc", box_matrix(GRID_W, window), lattice, precision=lax.Precision.HIGHEST
    )
    return jnp.einsum(
        "ab,bjc->ajc",
        box_matrix(lattice.shape[0], window),
        across,
        precision=lax.Precision.HIGHEST,
    )


def pooled_differences(channels, channel_offset):
    tokens_here, extent = channels.shape
    lattice = channels.reshape(tokens_here // GRID_W, GRID_W, extent)
    if GC % extent == 0:
        result = smooth(lattice, jnp.asarray(WINDOWS, jnp.int32)[channel_offset // GC])
    else:
        group_of = (channel_offset + jnp.arange(extent, dtype=jnp.int32)) // GC
        result = jnp.zeros_like(lattice)
        for group in range(GROUPS):
            result = jnp.where(
                (group_of == group)[None, None, :], smooth(lattice, WINDOWS[group]), result
            )
    return (result - lattice).reshape(tokens_here, extent).astype(jnp.bfloat16)


class Grid:
    def __init__(self, fs, tp):
        self.ys = max(tp // 2, 1)
        self.zs = fs // self.ys
        index = lax.axis_index("fs")
        self.z, self.y = index // self.ys, index % self.ys

    def gather(self, block):
        rows = []
        for s in range(self.zs):
            pairs = [
                (z * self.ys + y, (z + s) % self.zs * self.ys + y)
                for z in range(self.zs)
                for y in range(self.ys)
            ]
            rows.append(lax.ppermute(block, "fs", pairs) if s else block)
        found = []
        for s, row in enumerate(rows):
            for t in range(self.ys):
                pairs = [
                    (z * self.ys + y, z * self.ys + (y + t) % self.ys)
                    for z in range(self.zs)
                    for y in range(self.ys)
                ]
                item = lax.ppermute(row, "fs", pairs) if t else row
                index = lax.rem(self.z - s + self.zs, self.zs) * self.ys + lax.rem(
                    self.y - t + self.ys, self.ys
                )
                found.append((index, item))
        return found


def stack(pieces):
    shape = (len(pieces),) + pieces[0][1].shape
    result = jnp.zeros(shape, pieces[0][1].dtype)
    for index, item in pieces:
        result = lax.dynamic_update_index_in_dim(result, item, index, 0)
    return result


def rows_of(pieces):
    whole = stack(pieces)
    return whole.reshape(whole.shape[0] * whole.shape[1], whole.shape[2])


def fold_rows(features, gain, weights):
    widened = lax.all_gather(features, "tp", axis=1, tiled=True)
    widened = widened.astype(jnp.float32)
    inverse_rms = lax.rsqrt(jnp.mean(widened * widened, axis=1) + EPSILON)[:, None]
    scaled = (widened * gain).astype(jnp.bfloat16)
    return tuple(
        jnp.dot(scaled, weight, preferred_element_type=jnp.float32) * inverse_rms
        for weight in weights
    )


def column_product(hidden, pieces):
    terms = stack(
        [
            (index, jnp.dot(hidden, item, preferred_element_type=jnp.float32).astype(jnp.bfloat16))
            for index, item in pieces
        ]
    )
    mine = lax.psum_scatter(terms, "tp", scatter_dimension=0, tiled=True)
    return mine.transpose(1, 0, 2).reshape(hidden.shape[0], -1).astype(jnp.float32)


def low(weight, scale=None):
    weight = weight.astype(jnp.bfloat16)
    if scale is None:
        return weight
    return (weight.astype(jnp.float32) * scale).astype(jnp.bfloat16)


def general(mesh):
    fs, tp = mesh.shape["fs"], mesh.shape["tp"]

    def layer(
        tokens,
        mix_gain,
        in_weight,
        in_scale,
        out_weight,
        out_scale,
        ffn_gain,
        gate_weight,
        gate_scale,
        up_weight,
        up_scale,
        down_weight,
        down_scale,
    ):
        grid = Grid(fs, tp)
        wide = gate_weight.shape[1]
        both_pieces = grid.gather(jnp.concatenate([low(gate_weight), low(up_weight)], axis=1))
        down_pieces = grid.gather(low(down_weight, down_scale))
        small = lax.all_gather(
            jnp.stack([low(in_weight), low(out_weight, out_scale)]), "fs", axis=0
        )
        in_full = small[:, 0].reshape(-1, in_weight.shape[1])
        out_pieces = [(j, small[j, 1]) for j in range(fs)]
        (channels,) = fold_rows(tokens, mix_gain, (in_full,))
        channels = channels * in_scale
        pooled = pooled_differences(channels, lax.axis_index("tp") * channels.shape[1])
        mixed = column_product(pooled, out_pieces)
        residual = (tokens.astype(jnp.float32) + mixed).astype(jnp.bfloat16)
        (both,) = fold_rows(residual, ffn_gain, (rows_of(both_pieces),))
        gate_value = both[:, :wide] * gate_scale
        up_value = both[:, wide:] * up_scale
        hidden = (jax.nn.silu(gate_value) * up_value).astype(jnp.bfloat16)
        channel_out = column_product(hidden, down_pieces)
        return (residual.astype(jnp.float32) + channel_out).astype(jnp.bfloat16)

    return jax.shard_map(
        layer, mesh=mesh, in_specs=IN_SPECS, out_specs=P("fs", "tp"), check_vma=False
    )


class Place:
    def __init__(self):
        index, column = lax.axis_index("fs"), lax.axis_index("tp")
        z, self.y = index // 2, index % 2
        self.zh, self.zl = z // 2, z % 2
        self.x, self.c = column // 2, column % 2
        self.index, self.column = index, column
        self.to_x = {"tp": (1 - self.x) * 2 + self.c}
        self.to_c = {"tp": self.x * 2 + 1 - self.c}
        self.to_y = {"fs": z * 2 + 1 - self.y}
        self.to_zl = {"fs": (self.zh * 2 + 1 - self.zl) * 2 + self.y}
        self.to_zh = {"fs": ((1 - self.zh) * 2 + self.zl) * 2 + self.y}

    def slot(self, dh, dl, dy):
        zh, zl, y = (self.zh + dh) % 2, (self.zl + dl) % 2, (self.y + dy) % 2
        return (zh * 2 + zl) * 2 + y


class Mail:
    def __init__(self):
        self.started = []

    def send(self, source, target, send_sem, recv_sem, device):
        copy = pltpu.make_async_remote_copy(
            src_ref=source,
            dst_ref=target,
            send_sem=send_sem,
            recv_sem=recv_sem,
            device_id=device,
            device_id_type=pl.DeviceIdType.MESH,
        )
        copy.start()
        self.started.append(copy)

    def arrived(self, target, recv_sem):
        pltpu.make_async_copy(target, target, recv_sem).wait()

    def close(self):
        for copy in self.started:
            copy.wait_send()
        self.started = []


class Gather:
    def __init__(self, mail, place, kind, target, sends, recvs):
        self.mail, self.place, self.kind = mail, place, kind
        self.target, self.sends, self.recvs = target, sends, recvs
        self.count = 0

    def pass_on(self, source, slot, device):
        self.mail.send(
            source,
            self.target(slot),
            self.sends.at[self.kind, self.count],
            self.recvs.at[self.kind, slot],
            device,
        )
        self.count += 1

    def forward(self, slot, *devices):
        self.mail.arrived(self.target(slot), self.recvs.at[self.kind, slot])
        for device in devices:
            self.pass_on(self.target(slot), slot, device)

    def keep(self, own, sem):
        copy = pltpu.make_async_copy(own, self.target(self.place.index), sem)
        copy.start()
        return copy

    def rows_y(self):
        for dh, dl in ((0, 0), (0, 1), (1, 0), (1, 1)):
            self.forward(self.place.slot(dh, dl, 1))


class WholeGather(Gather):
    def start(self, own):
        p = self.place
        self.pass_on(own, p.index, p.to_zh)
        self.pass_on(own, p.index, p.to_zl)
        self.pass_on(own, p.index, p.to_y)

    def on_zh(self):
        p = self.place
        self.forward(p.slot(1, 0, 0), p.to_zl, p.to_y)

    def on_zl(self):
        p = self.place
        self.forward(p.slot(0, 1, 0), p.to_y)
        self.forward(p.slot(1, 1, 0), p.to_y)


class HalfGather(Gather):
    def start(self, own, other):
        p = self.place
        self.pass_on(other, p.index, p.to_zl)
        self.pass_on(own, p.index, p.to_zh)
        self.pass_on(own, p.index, p.to_y)

    def on_zl(self):
        p = self.place
        self.forward(p.slot(0, 1, 0), p.to_zh, p.to_y)

    def on_zh(self, dl):
        p = self.place
        self.forward(p.slot(1, dl, 0), p.to_y)


def lanes(start, size):
    return pl.ds(pl.multiple_of(start, 128), size)


def fused(
    tok, w_in, w_out, w_gu, w_dn, out,
    tokens, res, in_all, out_all, gu_all, dn_all, hid, mask, chan, high, low_part, pooled,
    mix_cs, mix_cr, mix_own, mix_xs, mix_xr,
    sum_cs, sum_cr, sum_xs, sum_xr, sum_zs, sum_zr, inv, done,
    local_sem, w_send, w_recv, t_send, t_recv, r_send, r_recv, m_send, m_recv, s_send, s_recv,
):
    rows, features = tokens.shape
    cols = tok.shape[1]
    block = w_in.shape[0]
    half = gu_all.shape[2] // 2
    chunk = rows // 4
    tall = rows // 2
    p, mail = Place(), Mail()

    def kept(kind):
        return {
            0: lambda j: in_all.at[pl.ds(pl.multiple_of(j * block, 16), block), :],
            1: lambda j: out_all.at[j],
            2: lambda j: gu_all.at[0, pl.ds(pl.multiple_of(j * block, 16), block), :],
            3: lambda j: gu_all.at[1, pl.ds(pl.multiple_of(j * block, 16), block), :],
            4: lambda j: dn_all.at[j],
        }[kind]

    g_in, g_out = (WholeGather(mail, p, k, kept(k), w_send, w_recv) for k in (0, 1))
    g_gu = [HalfGather(mail, p, 2 + q, kept(2 + q), w_send, w_recv) for q in (0, 1)]
    g_dn = HalfGather(mail, p, 4, kept(4), w_send, w_recv)

    def piece(k):
        return pl.ds(k * chunk, chunk)

    def column_of(dx, dc):
        return ((p.x + dx) % 2) * 2 + (p.c + dc) % 2

    g_in.start(w_in)
    for k in range(4):
        own = tok.at[piece(k), :]
        at = tokens.at[piece(k), lanes(p.column * cols, cols)]
        mail.send(own, at, t_send.at[0, k], t_recv.at[p.column, k], p.to_x)
        mail.send(own, at, t_send.at[1, k], t_recv.at[p.column, k], p.to_c)
    g_out.start(w_out)
    copies = [
        pltpu.make_async_copy(tok, tokens.at[:, lanes(p.column * cols, cols)], local_sem.at[0])
    ]
    copies[0].start()
    copies.append(g_in.keep(w_in, local_sem.at[1]))
    copies.append(g_out.keep(w_out, local_sem.at[2]))
    for q in (0, 1):
        copies.append(g_gu[q].keep(w_gu.at[p.zl, q], local_sem.at[3 + q]))
    copies.append(g_dn.keep(w_dn.at[p.zl], local_sem.at[5]))

    window = lax.shift_left(2, p.column * block // GC)
    below = window // 2
    above = window - below

    def mask_rows(i, _):
        cell = i * chunk // 2 + lax.broadcasted_iota(jnp.int32, (chunk // 2, rows), 0)
        other = lax.broadcasted_iota(jnp.int32, (chunk // 2, rows), 1)
        dr = other // GRID_W - cell // GRID_W
        dc = other % GRID_W - cell % GRID_W
        inside = (dr >= -below) & (dr < above) & (dc >= -below) & (dc < above)
        at = pl.ds(pl.multiple_of(i * (chunk // 2), 16), chunk // 2)
        mask[at, :] = jnp.where(inside, 1.0, 0.0).astype(jnp.bfloat16)
        return 0

    lax.fori_loop(0, 8, mask_rows, 0)

    g_in.on_zh()
    g_out.on_zh()
    g_in.on_zl()
    g_out.on_zl()
    for q in (0, 1):
        g_gu[q].start(w_gu.at[p.zl, q], w_gu.at[1 - p.zl, q])

    def token_at(column, k):
        return tokens.at[piece(k), lanes(column * cols, cols)]

    for k in range(4):
        column = column_of(1, 0)
        mail.arrived(token_at(column, k), t_recv.at[column, k])
        mail.send(
            token_at(column, k), token_at(column, k), t_send.at[2, k], t_recv.at[column, k], p.to_c
        )
    for copy in copies:
        copy.wait()
    for dx in (0, 1):
        for k in range(4):
            column = column_of(dx, 1)
            mail.arrived(token_at(column, k), t_recv.at[column, k])
    g_in.rows_y()

    def channel_rows(i, _):
        at = pl.ds(pl.multiple_of(i * chunk, 16), chunk)
        wide = tokens[at, :]
        square = wide.astype(jnp.float32)
        scale = lax.rsqrt(jnp.sum(square * square, axis=1, keepdims=True) / features + EPSILON)
        value = jnp.dot(wide, in_all[...], preferred_element_type=jnp.float32) * scale
        chan[at, :] = value
        first = value.astype(jnp.bfloat16)
        high[at, :] = first
        low_part[at, :] = (value - first.astype(jnp.float32)).astype(jnp.bfloat16)
        return 0

    lax.fori_loop(0, 4, channel_rows, 0)

    def extent(position, length):
        upper = jnp.minimum(position + above, length)
        return upper - jnp.maximum(position - below, 0)

    def pool_rows(i, _):
        at = pl.ds(pl.multiple_of(i * chunk, 16), chunk)
        inside = mask[at, :]
        total = jnp.dot(inside, high[...], preferred_element_type=jnp.float32) + jnp.dot(
            inside, low_part[...], preferred_element_type=jnp.float32
        )
        cell = i * chunk + lax.broadcasted_iota(jnp.int32, (chunk, block), 0)
        cells = extent(cell // GRID_W, rows // GRID_W) * extent(cell % GRID_W, GRID_W)
        pooled[at, :] = (total / cells.astype(jnp.float32) - chan[at, :]).astype(jnp.bfloat16)
        return 0

    lax.fori_loop(0, 4, pool_rows, 0)

    g_gu[0].on_zl()
    g_out.rows_y()

    for k in range(4):
        part = pooled[piece(k), :]
        for dx in (0, 1):
            for dc in (0, 1):
                target = mix_own if dc == 0 else mix_cs
                for side in (0, 1):
                    j = column_of(dx, dc) * 2 + side
                    term = jnp.dot(part, out_all[j], preferred_element_type=jnp.float32)
                    target[k, dx, :, side * block:(side + 1) * block] = term.astype(jnp.bfloat16)
        mail.send(mix_cs.at[k], mix_cr.at[k], m_send.at[0, k], m_recv.at[0, k], p.to_c)

    def both(k, dx):
        return mix_own[k, dx].astype(jnp.float32) + mix_cr[k, dx].astype(jnp.float32)

    for k in range(4):
        mail.arrived(mix_cr.at[k], m_recv.at[0, k])
        mix_xs[k] = both(k, 1).astype(jnp.bfloat16)
        mail.send(mix_xs.at[k], mix_xr.at[k], m_send.at[1, k], m_recv.at[1, k], p.to_x)
    g_gu[1].on_zl()
    g_dn.start(w_dn.at[p.zl], w_dn.at[1 - p.zl])

    def res_at(dz, column, k):
        return res.at[(p.zl + dz) % 2, piece(k), lanes(column * cols, cols)]

    def res_send(dz, column, k, lane, device):
        here = res_at(dz, column, k)
        sem = ((p.zl + dz) % 2) * 4 + column
        mail.send(here, here, r_send.at[lane, k], r_recv.at[sem, k], device)

    def res_wait(dz, column, k):
        sem = ((p.zl + dz) % 2) * 4 + column
        mail.arrived(res_at(dz, column, k), r_recv.at[sem, k])

    for k in range(4):
        mail.arrived(mix_xr.at[k], m_recv.at[1, k])
        mine = lanes(p.column * cols, cols)
        total = both(k, 0) + mix_xr[k].astype(jnp.float32)
        total = total + tokens[piece(k), mine].astype(jnp.float32)
        res[p.zl, piece(k), mine] = total.astype(jnp.bfloat16)
        res_send(0, p.column, k, 0, p.to_x)
        res_send(0, p.column, k, 1, p.to_zl)
        res_send(0, p.column, k, 2, p.to_c)
        if k == 1:
            g_gu[0].on_zh(0)

    for k in range(4):
        res_wait(1, p.column, k)
        if k < 2:
            res_send(1, p.column, k, 3, p.to_x)
        res_send(1, p.column, k, 4, p.to_c)
    g_gu[1].on_zh(0)
    across = column_of(1, 0)
    for k in range(4):
        res_wait(0, across, k)
        if k >= 2:
            res_send(0, across, k, 3, p.to_zl)
        res_send(0, across, k, 5, p.to_c)
    g_gu[0].on_zh(1)
    g_dn.on_zl()
    for k in range(4):
        res_wait(1, across, k)
        res_send(1, across, k, 6, p.to_c)
    g_gu[1].on_zh(1)
    for dz in (0, 1):
        for dx in (0, 1):
            for k in range(4):
                res_wait(dz, column_of(dx, 1), k)

    def norm_rows(i, _):
        at = pl.ds(pl.multiple_of((i % 4) * chunk, 16), chunk)
        square = res[i // 4, at, :].astype(jnp.float32)
        scale = lax.rsqrt(jnp.sum(square * square, axis=1, keepdims=True) / features + EPSILON)
        inv[i // 4, at, :] = jnp.broadcast_to(scale, (chunk, inv.shape[2]))
        return 0

    lax.fori_loop(0, 8, norm_rows, 0)
    for q in (0, 1):
        g_gu[q].rows_y()

        def hidden_rows(i, _):
            at = pl.ds(pl.multiple_of((i % 4) * chunk, 16), chunk)
            scale = inv[i // 4, at, :1]
            value = jnp.dot(
                res[i // 4, at, :], gu_all[q], preferred_element_type=jnp.float32
            ) * scale
            gate, up = value[:, :half], value[:, half:]
            unit = gate / (1.0 + jnp.exp(-gate)) * up
            hid[i // 4, at, q * half:(q + 1) * half] = unit.astype(jnp.bfloat16)
            return 0

        lax.fori_loop(0, 8, hidden_rows, 0)
        if q == 0:
            g_dn.on_zh(0)
    g_dn.on_zh(1)

    def sum_own(u, dx):
        return tokens.at[pl.ds((u % 2) * tall, tall), pl.ds((u // 2 * 2 + dx) * block, block)]

    def stage_core(u):
        dy, dz, k = u // 4, 1 - u // 2 % 2, u % 2
        part = hid[(p.zl + dz) % 2, pl.ds(k * tall, tall), :]
        for dx in (0, 1):
            for dc in (0, 1):
                j = column_of(dx, dc) * 2 + (p.y + dy) % 2
                term = jnp.dot(part, dn_all[j], preferred_element_type=jnp.float32)
                if dc == 0:
                    sum_own(u, dx)[...] = term.astype(jnp.bfloat16)
                else:
                    sum_cs[u, dx] = term.astype(jnp.bfloat16)
        mail.send(sum_cs.at[u], sum_cr.at[u], s_send.at[0, u], s_recv.at[0, u], p.to_c)

    def pair(u, dx):
        return sum_own(u, dx)[...].astype(jnp.float32) + sum_cr[u, dx].astype(jnp.float32)

    def stage_x(u):
        mail.arrived(sum_cr.at[u], s_recv.at[0, u])
        sum_xs[u] = pair(u, 1).astype(jnp.bfloat16)
        mail.send(sum_xs.at[u], sum_xr.at[u], s_send.at[1, u], s_recv.at[1, u], p.to_x)

    mail.close()
    for u in range(8):
        if u == 4:
            g_dn.rows_y()
        stage_core(u)
        if u:
            stage_x(u - 1)
    stage_x(7)

    for u in range(8):
        dy, dz, k = u // 4, 1 - u // 2 % 2, u % 2
        mail.arrived(sum_xr.at[u], s_recv.at[1, u])
        total = pair(u, 0) + sum_xr[u].astype(jnp.float32)
        n = dy * 2 + k
        if dz:
            sum_zs[n] = total.astype(jnp.bfloat16)
            mail.send(sum_zs.at[n], sum_zr.at[n], s_send.at[2, n], s_recv.at[2, n], p.to_zl)
        else:
            mail.arrived(sum_zr.at[n], s_recv.at[2, n])
            side = (p.y + dy) % 2 * block
            at = pl.ds(k * tall, tall)
            total = total + sum_zr[n].astype(jnp.float32)
            total = total + res[p.zl, at, lanes(p.column * cols + side, block)].astype(jnp.float32)
            done[at, lanes(side, block)] = total.astype(jnp.bfloat16)
    copy = pltpu.make_async_copy(done, out, local_sem.at[0])
    copy.start()
    mail.close()
    copy.wait()


def paired(mesh):
    fs, tp = mesh.shape["fs"], mesh.shape["tp"]

    def local(
        tokens,
        mix_gain,
        in_weight,
        in_scale,
        out_weight,
        out_scale,
        ffn_gain,
        gate_weight,
        gate_scale,
        up_weight,
        up_scale,
        down_weight,
        down_scale,
    ):
        rows, cols = tokens.shape
        depth, block = in_weight.shape
        wide = gate_weight.shape[1]
        start = lax.axis_index("fs") * depth
        mix_rows = lax.dynamic_slice(mix_gain, (start,), (depth,))[:, None]
        ffn_rows = lax.dynamic_slice(ffn_gain, (start,), (depth,))[:, None]
        w_in = low(in_weight, mix_rows * in_scale)
        w_out = low(out_weight, out_scale)
        quarters = [
            low(weight, ffn_rows * scale).reshape(depth, 2, 2, wide // 4)
            for weight, scale in ((gate_weight, gate_scale), (up_weight, up_scale))
        ]
        w_gu = jnp.concatenate(quarters, axis=3).transpose(1, 2, 0, 3)
        w_dn = low(down_weight, down_scale).reshape(2, wide // 2, block)
        features = cols * tp
        low_type = jnp.bfloat16
        tall = rows // 2
        buffers = [
            ((rows, features), low_type),
            ((2, rows, features), low_type),
            ((features, block), low_type),
            ((fs, block, block), low_type),
            ((2, features, wide // 2), low_type),
            ((fs, wide // 2, block), low_type),
            ((2, rows, wide // 2), low_type),
            ((rows, rows), low_type),
            ((rows, block), jnp.float32),
            ((rows, block), low_type),
            ((rows, block), low_type),
            ((rows, block), low_type),
            ((4, 2, rows // 4, cols), low_type),
            ((4, 2, rows // 4, cols), low_type),
            ((4, 2, rows // 4, cols), low_type),
            ((4, rows // 4, cols), low_type),
            ((4, rows // 4, cols), low_type),
            ((8, 2, tall, block), low_type),
            ((8, 2, tall, block), low_type),
            ((8, tall, block), low_type),
            ((8, tall, block), low_type),
            ((4, tall, block), low_type),
            ((4, tall, block), low_type),
            ((2, rows, 128), jnp.float32),
            ((rows, cols), low_type),
        ]
        semaphores = [(6,), (5, 7), (5, fs), (3, 4), (tp, 4), (7, 4), (2 * tp, 4), (2, 4), (2, 4)]
        semaphores += [(3, 8), (3, 8)]
        anywhere = pl.BlockSpec(memory_space=pl.ANY)
        return pl.pallas_call(
            fused,
            out_shape=jax.ShapeDtypeStruct((rows, cols), low_type),
            in_specs=[anywhere] * 5,
            out_specs=anywhere,
            scratch_shapes=[pltpu.VMEM(shape, kind) for shape, kind in buffers]
            + [pltpu.SemaphoreType.DMA(shape) for shape in semaphores],
            compiler_params=pltpu.CompilerParams(
                has_side_effects=True, vmem_limit_bytes=67043328
            ),
        )(tokens, w_in, w_out, w_gu, w_dn)

    return jax.shard_map(
        local, mesh=mesh, in_specs=IN_SPECS, out_specs=P("fs", "tp"), check_vma=False
    )


def solution(mesh):
    fs, tp = mesh.shape["fs"], mesh.shape["tp"]
    xs = max(tp // 2, 1)
    return paired(mesh) if (xs, fs // xs) == (2, 4) else general(mesh)
```

profile of v0, /device:TPU:22, one launch (start us, length us, event | category | flops | bytes accessed | tf_op | source)
XLA Modules:
  0.0 231.1 jit_solution(873370609038372797)
XLA Ops:
  0.0 0.8 dynamic_slice.6
  0.8 0.8 dynamic_slice.7
  1.5 0.0 copy-start
  1.5 1.9 multiply_convert_fusion.3
  3.5 1.7 copy.14
  5.1 0.0 copy-done
  5.1 0.0 copy-start.2
  5.2 0.0 copy-start.3
  5.2 0.3 copy.15
  5.4 0.4 copy-done.2
  5.8 0.0 copy-done.3
  5.9 0.5 multiply_convert_fusion.2
  6.3 0.4 copy.16
  6.7 0.4 copy.17
  7.1 0.0 copy-start.1
  7.1 0.0 copy-start.4
  7.1 1.3 maximum_bitcast_fusion.w_gu
  8.4 0.7 copy-done.1
  9.0 0.0 copy-done.4
  9.0 1.0 multiply_convert_fusion
  10.1 218.7 %shard_map.127 = bf16[1024,512]{1,0:T(8,128)(2,1)} custom-call(bf16[1024,512]{1,0:T(8,128)(2,1)} %tok.1, bf16[256,256]{1,0:T(8,128)(2,1)} %get-tuple-element.8.w_in, bf16[256,256]{1,0:T(8,128)(2,1)} %get-tuple-element.7.w_out, bf16[2,2,256,768]{3,2,1,0:T(8,128)(2,1)} %maximum_bitcast_fusion.w_gu, bf16[2,768,256]{2,1,0:T(8,128)(2,1)} %bitcast.5), custom_call_target="tpu_custom_call" | custom-call | tf_op jit(solution)/shard_map/pallas_call | solution.py:635
  228.8 2.3 copy.19
Async XLA Ops:
  1.5 3.6 %copy-start = (f32[256,1536]{1,0:T(8,128)S(1)}, f32[256,1536]{1,0:T(8,128)}, u32[]{:S(2)}) copy-start(f32[256,1536]{1,0:T(8,128)} %param.22) | copy-start | bytes 4718596
  5.1 0.7 copy-start.2
  5.2 0.7 copy-start.3
  7.1 2.0 copy-start.1
  7.1 2.0 copy-start.4
where the time goes:
time: 234 us; the launch traced here: 231 us
  Pallas kernels  219 us (94%)
  local copies, waits for them, and re-layouts  7.55 us (3%)
  other arithmetic  4.71 us (2%)
    pallas_call x1, Pallas kernels, local(): pl.pallas_call(fused, out_shape=jax.ShapeDtypeStruct((rows, cols), low_ty...  219 us
    unnamed x13, local copies, waits for them, and re-layouts  5.32 us

commit v1 on v0

--- a/solution.py
+++ b/solution.py
@@ -215,14 +215,18 @@
         )
         copy.start()
         self.started.append(copy)
+        return copy
 
     def arrived(self, target, recv_sem):
         pltpu.make_async_copy(target, target, recv_sem).wait()
 
+    def settle(self, copies):
+        for copy in copies:
+            copy.wait_send()
+        self.started = [copy for copy in self.started if all(copy is not c for c in copies)]
+
     def close(self):
-        for copy in self.started:
-            copy.wait_send()
-        self.started = []
+        self.settle(self.started)
 
 
 class Gather:
@@ -246,11 +250,6 @@
         for device in devices:
             self.pass_on(self.target(slot), slot, device)
 
-    def keep(self, own, sem):
-        copy = pltpu.make_async_copy(own, self.target(self.place.index), sem)
-        copy.start()
-        return copy
-
     def rows_y(self):
         for dh, dl in ((0, 0), (0, 1), (1, 0), (1, 1)):
             self.forward(self.place.slot(dh, dl, 1))
@@ -274,11 +273,18 @@
 
 
 class HalfGather(Gather):
-    def start(self, own, other):
-        p = self.place
-        self.pass_on(other, p.index, p.to_zl)
-        self.pass_on(own, p.index, p.to_zh)
-        self.pass_on(own, p.index, p.to_y)
+    def start_zl(self, other):
+        self.pass_on(other, self.place.index, self.place.to_zl)
+
+    def start_zh(self, own):
+        self.pass_on(own, self.place.index, self.place.to_zh)
+
+    def start_y(self, own):
+        self.pass_on(own, self.place.index, self.place.to_y)
+
+    def start(self, own):
+        self.start_zh(own)
+        self.start_y(own)
 
     def on_zl(self):
         p = self.place
@@ -294,15 +300,19 @@
 
 
 def fused(
-    tok, w_in, w_out, w_gu, w_dn, out,
+    tok, w_in, w_out, w_gate, w_up, w_down,
+    gain_mix, gain_ffn, s_in, s_out, s_gate, s_up, s_down, out,
     tokens, res, in_all, out_all, gu_all, dn_all, hid, mask, chan, high, low_part, pooled,
     mix_cs, mix_cr, mix_own, mix_xs, mix_xr,
-    sum_cs, sum_cr, sum_xs, sum_xr, sum_zs, sum_zr, inv, done,
-    local_sem, w_send, w_recv, t_send, t_recv, r_send, r_recv, m_send, m_recv, s_send, s_recv,
+    sum_cs, sum_cr, sum_xs, sum_xr, sum_zs, sum_zr, done,
+    f_in, f_out, f_gate, f_up, f_down, gu_other, dn_other,
+    local_sem, w_send, w_recv, t_send, t_recv, r_send, r_recv, m_send, m_recv,
+    c_send, c_recv, x_send, x_recv, z_send, z_recv,
 ):
     rows, features = tokens.shape
     cols = tok.shape[1]
     block = w_in.shape[0]
+    unit_hidden = dn_all.shape[1]
     half = gu_all.shape[2] // 2
     chunk = rows // 4
     tall = rows // 2
@@ -327,22 +337,54 @@
     def column_of(dx, dc):
         return ((p.x + dx) % 2) * 2 + (p.c + dc) % 2
 
-    g_in.start(w_in)
+    copies = [
+        pltpu.make_async_copy(source, target, local_sem.at[n])
+        for n, (source, target) in enumerate((
+            (w_in, f_in),
+            (w_out, f_out),
+            (tok, tokens.at[:, lanes(p.column * cols, cols)]),
+            (w_gate, f_gate),
+            (w_up, f_up),
+            (w_down, f_down),
+        ))
+    ]
+    for copy in copies:
+        copy.start()
+    barrier = pltpu.get_barrier_semaphore()
+    for device in (p.to_c, p.to_x, p.to_y, p.to_zl, p.to_zh):
+        pl.semaphore_signal(
+            barrier, inc=1, device_id=device, device_id_type=pl.DeviceIdType.MESH
+        )
+    pl.semaphore_wait(barrier, 5)
     for k in range(4):
         own = tok.at[piece(k), :]
         at = tokens.at[piece(k), lanes(p.column * cols, cols)]
         mail.send(own, at, t_send.at[0, k], t_recv.at[p.column, k], p.to_x)
         mail.send(own, at, t_send.at[1, k], t_recv.at[p.column, k], p.to_c)
-    g_out.start(w_out)
-    copies = [
-        pltpu.make_async_copy(tok, tokens.at[:, lanes(p.column * cols, cols)], local_sem.at[0])
-    ]
-    copies[0].start()
-    copies.append(g_in.keep(w_in, local_sem.at[1]))
-    copies.append(g_out.keep(w_out, local_sem.at[2]))
+
+    def rounded(weight, scale):
+        weight = weight.astype(jnp.bfloat16).astype(jnp.float32)
+        return (weight * scale[None, :]).astype(jnp.bfloat16)
+
+    copies[0].wait()
+    kept(0)(p.index)[...] = rounded(f_in[...], s_in[...])
+    g_in.start(kept(0)(p.index))
+    copies[1].wait()
+    kept(1)(p.index)[...] = rounded(f_out[...], s_out[...])
+    g_out.start(kept(1)(p.index))
+    for copy in copies[3:]:
+        copy.wait()
     for q in (0, 1):
-        copies.append(g_gu[q].keep(w_gu.at[p.zl, q], local_sem.at[3 + q]))
-    copies.append(g_dn.keep(w_dn.at[p.zl], local_sem.at[5]))
+        for own in (True, False):
+            target = kept(2 + q)(p.index) if own else gu_other.at[q]
+            at = lanes(((p.zl if own else 1 - p.zl) * 2 + q) * half, half)
+            target[:, :half] = rounded(f_gate[:, at], s_gate[at])
+            target[:, half:] = rounded(f_up[:, at], s_up[at])
+    for own in (True, False):
+        target = kept(4)(p.index) if own else dn_other
+        at = (p.zl if own else 1 - p.zl) * unit_hidden
+        at = pl.ds(pl.multiple_of(at, 16), unit_hidden)
+        target[...] = rounded(f_down[at, :], s_down[...])
 
     window = lax.shift_left(2, p.column * block // GC)
     below = window // 2
@@ -365,30 +407,35 @@
     g_in.on_zl()
     g_out.on_zl()
     for q in (0, 1):
-        g_gu[q].start(w_gu.at[p.zl, q], w_gu.at[1 - p.zl, q])
+        g_gu[q].start_zl(gu_other.at[q])
+    for q in (0, 1):
+        g_gu[q].start(kept(2 + q)(p.index))
+    g_dn.start_y(kept(4)(p.index))
 
     def token_at(column, k):
         return tokens.at[piece(k), lanes(column * cols, cols)]
 
+    passed = []
     for k in range(4):
         column = column_of(1, 0)
-        mail.arrived(token_at(column, k), t_recv.at[column, k])
-        mail.send(
-            token_at(column, k), token_at(column, k), t_send.at[2, k], t_recv.at[column, k], p.to_c
-        )
-    for copy in copies:
-        copy.wait()
+        here = token_at(column, k)
+        mail.arrived(here, t_recv.at[column, k])
+        passed.append(mail.send(here, here, t_send.at[2, k], t_recv.at[column, k], p.to_c))
+    copies[2].wait()
     for dx in (0, 1):
         for k in range(4):
             column = column_of(dx, 1)
             mail.arrived(token_at(column, k), t_recv.at[column, k])
     g_in.rows_y()
 
+    def normed(wide, gain):
+        square = wide * wide
+        scale = lax.rsqrt(jnp.sum(square, axis=1, keepdims=True) / features + EPSILON)
+        return (wide * gain[...][None, :]).astype(jnp.bfloat16), scale
+
     def channel_rows(i, _):
         at = pl.ds(pl.multiple_of(i * chunk, 16), chunk)
-        wide = tokens[at, :]
-        square = wide.astype(jnp.float32)
-        scale = lax.rsqrt(jnp.sum(square * square, axis=1, keepdims=True) / features + EPSILON)
+        wide, scale = normed(tokens[at, :].astype(jnp.float32), gain_mix)
         value = jnp.dot(wide, in_all[...], preferred_element_type=jnp.float32) * scale
         chan[at, :] = value
         first = value.astype(jnp.bfloat16)
@@ -415,7 +462,6 @@
 
     lax.fori_loop(0, 4, pool_rows, 0)
 
-    g_gu[0].on_zl()
     g_out.rows_y()
 
     for k in range(4):
@@ -436,8 +482,6 @@
         mail.arrived(mix_cr.at[k], m_recv.at[0, k])
         mix_xs[k] = both(k, 1).astype(jnp.bfloat16)
         mail.send(mix_xs.at[k], mix_xr.at[k], m_send.at[1, k], m_recv.at[1, k], p.to_x)
-    g_gu[1].on_zl()
-    g_dn.start(w_dn.at[p.zl], w_dn.at[1 - p.zl])
 
     def res_at(dz, column, k):
         return res.at[(p.zl + dz) % 2, piece(k), lanes(column * cols, cols)]
@@ -460,107 +504,132 @@
         res_send(0, p.column, k, 0, p.to_x)
         res_send(0, p.column, k, 1, p.to_zl)
         res_send(0, p.column, k, 2, p.to_c)
-        if k == 1:
-            g_gu[0].on_zh(0)
-
-    for k in range(4):
+        if k > 1:
+            g_gu[k - 2].on_zl()
+    g_dn.start_zl(dn_other)
+    g_dn.start_zh(kept(4)(p.index))
+
+    across = column_of(1, 0)
+    for k in range(4):
+        res_wait(0, across, k)
+        res_send(0, across, k, 5, p.to_c)
         res_wait(1, p.column, k)
-        if k < 2:
-            res_send(1, p.column, k, 3, p.to_x)
+        res_send(1, p.column, k, 3, p.to_x)
         res_send(1, p.column, k, 4, p.to_c)
-    g_gu[1].on_zh(0)
-    across = column_of(1, 0)
-    for k in range(4):
-        res_wait(0, across, k)
-        if k >= 2:
-            res_send(0, across, k, 3, p.to_zl)
-        res_send(0, across, k, 5, p.to_c)
-    g_gu[0].on_zh(1)
+        g_gu[k % 2].on_zh(k // 2)
+    for k in range(4):
+        for dx in (0, 1):
+            res_wait(0, column_of(dx, 1), k)
+    for q in (0, 1):
+        g_gu[q].rows_y()
+
+    def hidden_rows(dz):
+        def body(i, _):
+            at = pl.ds(pl.multiple_of(i * chunk, 16), chunk)
+            z = (p.zl + dz) % 2
+            wide, scale = normed(res[z, at, :].astype(jnp.float32), gain_ffn)
+            for q in (0, 1):
+                value = jnp.dot(wide, gu_all[q], preferred_element_type=jnp.float32) * scale
+                gate, up = value[:, :half], value[:, half:]
+                unit = gate / (1.0 + jnp.exp(-gate)) * up
+                hid[z, at, q * half:(q + 1) * half] = unit.astype(jnp.bfloat16)
+            return 0
+
+        return body
+
+    lax.fori_loop(0, 4, hidden_rows(0), 0)
     g_dn.on_zl()
     for k in range(4):
         res_wait(1, across, k)
         res_send(1, across, k, 6, p.to_c)
-    g_gu[1].on_zh(1)
-    for dz in (0, 1):
+    for k in range(4):
         for dx in (0, 1):
-            for k in range(4):
-                res_wait(dz, column_of(dx, 1), k)
-
-    def norm_rows(i, _):
-        at = pl.ds(pl.multiple_of((i % 4) * chunk, 16), chunk)
-        square = res[i // 4, at, :].astype(jnp.float32)
-        scale = lax.rsqrt(jnp.sum(square * square, axis=1, keepdims=True) / features + EPSILON)
-        inv[i // 4, at, :] = jnp.broadcast_to(scale, (chunk, inv.shape[2]))
-        return 0
-
-    lax.fori_loop(0, 8, norm_rows, 0)
-    for q in (0, 1):
-        g_gu[q].rows_y()
-
-        def hidden_rows(i, _):
-            at = pl.ds(pl.multiple_of((i % 4) * chunk, 16), chunk)
-            scale = inv[i // 4, at, :1]
-            value = jnp.dot(
-                res[i // 4, at, :], gu_all[q], preferred_element_type=jnp.float32
-            ) * scale
-            gate, up = value[:, :half], value[:, half:]
-            unit = gate / (1.0 + jnp.exp(-gate)) * up
-            hid[i // 4, at, q * half:(q + 1) * half] = unit.astype(jnp.bfloat16)
-            return 0
-
-        lax.fori_loop(0, 8, hidden_rows, 0)
-        if q == 0:
-            g_dn.on_zh(0)
+            res_wait(1, column_of(dx, 1), k)
+    lax.fori_loop(0, 4, hidden_rows(1), 0)
+    g_dn.on_zh(0)
     g_dn.on_zh(1)
+
+    mail.settle(passed)
 
     def sum_own(u, dx):
         return tokens.at[pl.ds((u % 2) * tall, tall), pl.ds((u // 2 * 2 + dx) * block, block)]
 
-    def stage_core(u):
-        dy, dz, k = u // 4, 1 - u // 2 % 2, u % 2
+    def unit(dy, dz, k):
+        return dy * 4 + dz * 2 + k
+
+    def pair(u, dx):
+        return sum_own(u, dx)[...].astype(jnp.float32) + sum_cr[u, dx].astype(jnp.float32)
+
+    def x_send_at(n):
+        mail.send(sum_xs.at[n], sum_xr.at[n], x_send.at[n], x_recv.at[n], p.to_x)
+
+    def z_send_at(n):
+        mail.send(sum_zs.at[n], sum_zr.at[n], z_send.at[n], z_recv.at[n], p.to_zl)
+
+    def stage_core(dy, dz, k):
+        u = unit(dy, dz, k)
         part = hid[(p.zl + dz) % 2, pl.ds(k * tall, tall), :]
-        for dx in (0, 1):
-            for dc in (0, 1):
+        for dc in (1, 0):
+            for dx in (0, 1):
                 j = column_of(dx, dc) * 2 + (p.y + dy) % 2
                 term = jnp.dot(part, dn_all[j], preferred_element_type=jnp.float32)
                 if dc == 0:
                     sum_own(u, dx)[...] = term.astype(jnp.bfloat16)
                 else:
                     sum_cs[u, dx] = term.astype(jnp.bfloat16)
-        mail.send(sum_cs.at[u], sum_cr.at[u], s_send.at[0, u], s_recv.at[0, u], p.to_c)
-
-    def pair(u, dx):
-        return sum_own(u, dx)[...].astype(jnp.float32) + sum_cr[u, dx].astype(jnp.float32)
-
-    def stage_x(u):
-        mail.arrived(sum_cr.at[u], s_recv.at[0, u])
-        sum_xs[u] = pair(u, 1).astype(jnp.bfloat16)
-        mail.send(sum_xs.at[u], sum_xr.at[u], s_send.at[1, u], s_recv.at[1, u], p.to_x)
-
-    mail.close()
-    for u in range(8):
-        if u == 4:
-            g_dn.rows_y()
-        stage_core(u)
-        if u:
-            stage_x(u - 1)
-    stage_x(7)
-
-    for u in range(8):
-        dy, dz, k = u // 4, 1 - u // 2 % 2, u % 2
-        mail.arrived(sum_xr.at[u], s_recv.at[1, u])
-        total = pair(u, 0) + sum_xr[u].astype(jnp.float32)
-        n = dy * 2 + k
-        if dz:
-            sum_zs[n] = total.astype(jnp.bfloat16)
-            mail.send(sum_zs.at[n], sum_zr.at[n], s_send.at[2, n], s_recv.at[2, n], p.to_zl)
-        else:
-            mail.arrived(sum_zr.at[n], s_recv.at[2, n])
-            side = (p.y + dy) % 2 * block
+            if dc:
+                mail.send(sum_cs.at[u], sum_cr.at[u], c_send.at[u], c_recv.at[u], p.to_c)
+
+    def stage_first(dy, dz, k):
+        u = unit(dy, dz, k)
+        mail.arrived(sum_cr.at[u], c_recv.at[u])
+        if k == 0:
+            n = dy * 3 + dz
+            sum_xs[n] = pair(u, 1).astype(jnp.bfloat16)
+            x_send_at(n)
+        elif dz == 1:
+            for dx in (1, 0):
+                n = dy * 3 + dx
+                sum_zs[n] = pair(u, dx).astype(jnp.bfloat16)
+                z_send_at(n)
+
+    def stage_second(dy):
+        n = dy * 3
+        mail.arrived(sum_xr.at[n + 1], x_recv.at[n + 1])
+        total = pair(unit(dy, 1, 0), 0) + sum_xr[n + 1].astype(jnp.float32)
+        sum_zs[n + 2] = total.astype(jnp.bfloat16)
+        z_send_at(n + 2)
+        mail.arrived(sum_zr.at[n + 1], z_recv.at[n + 1])
+        total = pair(unit(dy, 0, 1), 1) + sum_zr[n + 1].astype(jnp.float32)
+        sum_xs[n + 2] = total.astype(jnp.bfloat16)
+        x_send_at(n + 2)
+
+    def stage_last(dy):
+        n = dy * 3
+        side = (p.y + dy) % 2 * block
+        for k in (0, 1):
+            first, second = (n, n + 2) if k == 0 else (n + 2, n)
+            mail.arrived(sum_xr.at[first], x_recv.at[first])
+            mail.arrived(sum_zr.at[second], z_recv.at[second])
+            total = pair(unit(dy, 0, k), 0)
+            total = total + sum_xr[first].astype(jnp.float32) + sum_zr[second].astype(jnp.float32)
             at = pl.ds(k * tall, tall)
-            total = total + sum_zr[n].astype(jnp.float32)
             total = total + res[p.zl, at, lanes(p.column * cols + side, block)].astype(jnp.float32)
             done[at, lanes(side, block)] = total.astype(jnp.bfloat16)
+
+    order = [(1, 0), (1, 1), (0, 0), (0, 1)]
+    for dy in (0, 1):
+        if dy:
+            g_dn.rows_y()
+        for n, (dz, k) in enumerate(order):
+            stage_core(dy, dz, k)
+            if n:
+                stage_first(dy, *order[n - 1])
+        stage_first(dy, *order[3])
+    for dy in (0, 1):
+        stage_second(dy)
+    for dy in (0, 1):
+        stage_last(dy)
     copy = pltpu.make_async_copy(done, out, local_sem.at[0])
     copy.start()
     mail.close()
@@ -588,17 +657,6 @@
         rows, cols = tokens.shape
         depth, block = in_weight.shape
         wide = gate_weight.shape[1]
-        start = lax.axis_index("fs") * depth
-        mix_rows = lax.dynamic_slice(mix_gain, (start,), (depth,))[:, None]
-        ffn_rows = lax.dynamic_slice(ffn_gain, (start,), (depth,))[:, None]
-        w_in = low(in_weight, mix_rows * in_scale)
-        w_out = low(out_weight, out_scale)
-        quarters = [
-            low(weight, ffn_rows * scale).reshape(depth, 2, 2, wide // 4)
-            for weight, scale in ((gate_weight, gate_scale), (up_weight, up_scale))
-        ]
-        w_gu = jnp.concatenate(quarters, axis=3).transpose(1, 2, 0, 3)
-        w_dn = low(down_weight, down_scale).reshape(2, wide // 2, block)
         features = cols * tp
         low_type = jnp.bfloat16
         tall = rows // 2
@@ -622,27 +680,43 @@
             ((4, rows // 4, cols), low_type),
             ((8, 2, tall, block), low_type),
             ((8, 2, tall, block), low_type),
-            ((8, tall, block), low_type),
-            ((8, tall, block), low_type),
-            ((4, tall, block), low_type),
-            ((4, tall, block), low_type),
-            ((2, rows, 128), jnp.float32),
+            ((6, tall, block), low_type),
+            ((6, tall, block), low_type),
+            ((6, tall, block), low_type),
+            ((6, tall, block), low_type),
             ((rows, cols), low_type),
+            (in_weight.shape, jnp.float32),
+            (out_weight.shape, jnp.float32),
+            (gate_weight.shape, jnp.float32),
+            (up_weight.shape, jnp.float32),
+            (down_weight.shape, jnp.float32),
+            ((2, depth, wide // 2), low_type),
+            ((wide // 2, block), low_type),
         ]
         semaphores = [(6,), (5, 7), (5, fs), (3, 4), (tp, 4), (7, 4), (2 * tp, 4), (2, 4), (2, 4)]
-        semaphores += [(3, 8), (3, 8)]
+        semaphores += [(8,), (8,), (6,), (6,), (6,), (6,)]
         anywhere = pl.BlockSpec(memory_space=pl.ANY)
+        inside = pl.BlockSpec(memory_space=pltpu.VMEM)
+        vectors = (mix_gain, ffn_gain, in_scale, out_scale, gate_scale, up_scale, down_scale)
         return pl.pallas_call(
             fused,
             out_shape=jax.ShapeDtypeStruct((rows, cols), low_type),
-            in_specs=[anywhere] * 5,
+            in_specs=[anywhere] * 6 + [inside] * len(vectors),
             out_specs=anywhere,
             scratch_shapes=[pltpu.VMEM(shape, kind) for shape, kind in buffers]
             + [pltpu.SemaphoreType.DMA(shape) for shape in semaphores],
             compiler_params=pltpu.CompilerParams(
-                has_side_effects=True, vmem_limit_bytes=67043328
+                collective_id=0, has_side_effects=True, vmem_limit_bytes=67043328
             ),
-        )(tokens, w_in, w_out, w_gu, w_dn)
+        )(
+            tokens,
+            in_weight,
+            out_weight,
+            gate_weight,
+            up_weight,
+            down_weight,
+            *vectors,
+        )
 
     return jax.shard_map(
         local, mesh=mesh, in_specs=IN_SPECS, out_specs=P("fs", "tp"), check_vma=False

time: 234 us -> 186 us (0.79); the launches traced: 231 us -> 186 us
  Pallas kernels: 219 us -> 184 us
  local copies, waits for them, and re-layouts: 7.55 us -> 2.26 us
  other arithmetic: 4.71 us -> 0 us
    pallas_call x1, Pallas kernels: 219 us -> 184 us  [local(): pl.pallas_call(fused, out_shape=jax.ShapeDtypeStruct((rows, cols), low_ty...]
    convert_element_type x3 -> x0, other arithmetic: 3.43 us -> none  [low(): return (weight.astype(jnp.float32) * scale).astype(jnp.bfloat16)]
    unnamed x13 -> x1, local copies, waits for them, and re-layouts: 5.32 us -> 2.26 us
where the time goes in v1:
time: 186 us
  Pallas kernels  184 us (99%)
  local copies, waits for them, and re-layouts  2.26 us (1%)
    pallas_call x1, Pallas kernels, local(): pl.pallas_call(fused, out_shape=jax.ShapeDtypeStruct((rows, cols), low_ty...  184 us

profile of v1, /device:TPU:22, one launch (start us, length us, event | category | flops | bytes accessed | tf_op | source)
XLA Modules:
  0.0 185.9 jit_solution(14964183927741979804)
XLA Ops:
  0.0 183.6 %shard_map.127 = bf16[1024,512]{1,0:T(8,128)(2,1)} custom-call(bf16[1024,512]{1,0:T(8,128)(2,1)} %tok.1, f32[256,256]{1,0:T(8,128)} %w_in.1, f32[256,256]{1,0:T(8,128)} %w_out.1, f32[256,1536]{1,0:T(8,128)} %w_gate.1, f32[256,1536]{1,0:T(8,128)} %w_up.1, f32[1536,256]{1,0:T(8,128)} %w_down.1, f32[2048]{0:T(1024)} %gain_mix.1, f32[2048]{0:T(1024)} %gain_ffn.1, ...), custom_call_target="tpu_custom_call" | custom-call | tf_op jit(solution)/shard_map/pallas_call | solution.py:701
  183.6 2.3 %copy.15 = bf16[1024,512]{1,0:T(8,128)(2,1)} copy(bf16[1024,512]{1,0:T(8,128)(2,1)} %shard_map.127) | data formatting | bytes 2097152

commit v2 on v1

--- a/solution.py
+++ b/solution.py
@@ -282,10 +282,6 @@
     def start_y(self, own):
         self.pass_on(own, self.place.index, self.place.to_y)
 
-    def start(self, own):
-        self.start_zh(own)
-        self.start_y(own)
-
     def on_zl(self):
         p = self.place
         self.forward(p.slot(0, 1, 0), p.to_zh, p.to_y)
@@ -409,7 +405,9 @@
     for q in (0, 1):
         g_gu[q].start_zl(gu_other.at[q])
     for q in (0, 1):
-        g_gu[q].start(kept(2 + q)(p.index))
+        g_gu[q].start_zh(kept(2 + q)(p.index))
+    for q in (0, 1):
+        g_gu[q].start_y(kept(2 + q)(p.index))
     g_dn.start_y(kept(4)(p.index))
 
     def token_at(column, k):
@@ -510,13 +508,34 @@
     g_dn.start_zh(kept(4)(p.index))
 
     across = column_of(1, 0)
-    for k in range(4):
+
+    def on_x(k):
         res_wait(0, across, k)
         res_send(0, across, k, 5, p.to_c)
+
+    def on_z(k):
         res_wait(1, p.column, k)
         res_send(1, p.column, k, 3, p.to_x)
         res_send(1, p.column, k, 4, p.to_c)
-        g_gu[k % 2].on_zh(k // 2)
+
+    def on_both(k):
+        res_wait(1, across, k)
+        res_send(1, across, k, 6, p.to_c)
+
+    on_x(0)
+    g_gu[0].on_zh(0)
+    on_x(1)
+    g_gu[1].on_zh(0)
+    on_x(2)
+    on_z(0)
+    on_x(3)
+    on_z(1)
+    g_gu[0].on_zh(1)
+    on_z(2)
+    g_gu[1].on_zh(1)
+    on_z(3)
+    on_both(0)
+    on_both(1)
     for k in range(4):
         for dx in (0, 1):
             res_wait(0, column_of(dx, 1), k)
@@ -537,16 +556,17 @@
 
         return body
 
-    lax.fori_loop(0, 4, hidden_rows(0), 0)
+    lax.fori_loop(0, 1, hidden_rows(0), 0)
     g_dn.on_zl()
-    for k in range(4):
-        res_wait(1, across, k)
-        res_send(1, across, k, 6, p.to_c)
+    on_both(2)
+    lax.fori_loop(1, 3, hidden_rows(0), 0)
+    on_both(3)
+    lax.fori_loop(3, 4, hidden_rows(0), 0)
+    g_dn.on_zh(0)
     for k in range(4):
         for dx in (0, 1):
             res_wait(1, column_of(dx, 1), k)
     lax.fori_loop(0, 4, hidden_rows(1), 0)
-    g_dn.on_zh(0)
     g_dn.on_zh(1)
 
     mail.settle(passed)
@@ -604,6 +624,8 @@
         sum_xs[n + 2] = total.astype(jnp.bfloat16)
         x_send_at(n + 2)
 
+    results = []
+
     def stage_last(dy):
         n = dy * 3
         side = (p.y + dy) % 2 * block
@@ -615,7 +637,11 @@
             total = total + sum_xr[first].astype(jnp.float32) + sum_zr[second].astype(jnp.float32)
             at = pl.ds(k * tall, tall)
             total = total + res[p.zl, at, lanes(p.column * cols + side, block)].astype(jnp.float32)
-            done[at, lanes(side, block)] = total.astype(jnp.bfloat16)
+            here = (at, lanes(side, block))
+            done[here] = total.astype(jnp.bfloat16)
+            copy = pltpu.make_async_copy(done.at[here], out.at[here], local_sem.at[dy * 2 + k])
+            copy.start()
+            results.append(copy)
 
     order = [(1, 0), (1, 1), (0, 0), (0, 1)]
     for dy in (0, 1):
@@ -623,17 +649,17 @@
             g_dn.rows_y()
         for n, (dz, k) in enumerate(order):
             stage_core(dy, dz, k)
-            if n:
-                stage_first(dy, *order[n - 1])
-        stage_first(dy, *order[3])
+            if n > 1:
+                stage_first(dy, *order[n - 2])
+        for n in (2, 3):
+            stage_first(dy, *order[n])
     for dy in (0, 1):
         stage_second(dy)
     for dy in (0, 1):
         stage_last(dy)
-    copy = pltpu.make_async_copy(done, out, local_sem.at[0])
-    copy.start()
     mail.close()
-    copy.wait()
+    for copy in results:
+        copy.wait()
 
 
 def paired(mesh):

time: 186 us -> 177 us (0.952)
  Pallas kernels: 184 us -> 173 us
    pallas_call x1, Pallas kernels: 184 us -> 173 us  [local(): pl.pallas_call(fused, out_shape=jax.ShapeDtypeStruct((rows, cols), low_ty...]
where the time goes in v2:
time: 177 us; the launch traced here: 175 us
  Pallas kernels  173 us (98%)
  local copies, waits for them, and re-layouts  2.26 us (1%)
    pallas_call x1, Pallas kernels, local(): pl.pallas_call(fused, out_shape=jax.ShapeDtypeStruct((rows, cols), low_ty...  173 us

profile of v2, /device:TPU:22, one launch (start us, length us, event | category | flops | bytes accessed | tf_op | source)
XLA Modules:
  0.0 175.5 jit_solution(5647376536319546439)
XLA Ops:
  0.0 173.2 %shard_map.127 = bf16[1024,512]{1,0:T(8,128)(2,1)} custom-call(bf16[1024,512]{1,0:T(8,128)(2,1)} %tok.1, f32[256,256]{1,0:T(8,128)} %w_in.1, f32[256,256]{1,0:T(8,128)} %w_out.1, f32[256,1536]{1,0:T(8,128)} %w_gate.1, f32[256,1536]{1,0:T(8,128)} %w_up.1, f32[1536,256]{1,0:T(8,128)} %w_down.1, f32[2048]{0:T(1024)} %gain_mix.1, f32[2048]{0:T(1024)} %gain_ffn.1, ...), custom_call_target="tpu_custom_call" | custom-call | tf_op jit(solution)/shard_map/pallas_call | solution.py:727
  173.2 2.3 %copy.15 = bf16[1024,512]{1,0:T(8,128)(2,1)} copy(bf16[1024,512]{1,0:T(8,128)(2,1)} %shard_map.127) | data formatting | bytes 2097152

commit v3 on v2

--- a/solution.py
+++ b/solution.py
@@ -204,8 +204,8 @@
     def __init__(self):
         self.started = []
 
-    def send(self, source, target, send_sem, recv_sem, device):
-        copy = pltpu.make_async_remote_copy(
+    def make(self, source, target, send_sem, recv_sem, device):
+        return pltpu.make_async_remote_copy(
             src_ref=source,
             dst_ref=target,
             send_sem=send_sem,
@@ -213,6 +213,9 @@
             device_id=device,
             device_id_type=pl.DeviceIdType.MESH,
         )
+
+    def send(self, source, target, send_sem, recv_sem, device):
+        copy = self.make(source, target, send_sem, recv_sem, device)
         copy.start()
         self.started.append(copy)
         return copy
@@ -250,9 +253,10 @@
         for device in devices:
             self.pass_on(self.target(slot), slot, device)
 
-    def rows_y(self):
-        for dh, dl in ((0, 0), (0, 1), (1, 0), (1, 1)):
-            self.forward(self.place.slot(dh, dl, 1))
+    def rows_y(self, lows=(0, 1)):
+        for dl in lows:
+            for dh in (0, 1):
+                self.forward(self.place.slot(dh, dl, 1))
 
 
 class WholeGather(Gather):
@@ -505,7 +509,6 @@
         if k > 1:
             g_gu[k - 2].on_zl()
     g_dn.start_zl(dn_other)
-    g_dn.start_zh(kept(4)(p.index))
 
     across = column_of(1, 0)
 
@@ -531,23 +534,22 @@
     on_x(3)
     on_z(1)
     g_gu[0].on_zh(1)
+    g_dn.start_zh(kept(4)(p.index))
+    g_gu[1].on_zh(1)
     on_z(2)
-    g_gu[1].on_zh(1)
-    on_z(3)
     on_both(0)
     on_both(1)
     for k in range(4):
         for dx in (0, 1):
             res_wait(0, column_of(dx, 1), k)
-    for q in (0, 1):
-        g_gu[q].rows_y()
-
-    def hidden_rows(dz):
+    g_gu[0].rows_y()
+
+    def hidden_rows(dz, *halves):
         def body(i, _):
             at = pl.ds(pl.multiple_of(i * chunk, 16), chunk)
             z = (p.zl + dz) % 2
             wide, scale = normed(res[z, at, :].astype(jnp.float32), gain_ffn)
-            for q in (0, 1):
+            for q in halves:
                 value = jnp.dot(wide, gu_all[q], preferred_element_type=jnp.float32) * scale
                 gate, up = value[:, :half], value[:, half:]
                 unit = gate / (1.0 + jnp.exp(-gate)) * up
@@ -556,107 +558,150 @@
 
         return body
 
-    lax.fori_loop(0, 1, hidden_rows(0), 0)
+    lax.fori_loop(0, 4, hidden_rows(0, 0), 0)
+    on_z(3)
+    g_gu[1].rows_y()
+    lax.fori_loop(0, 2, hidden_rows(0, 1), 0)
     g_dn.on_zl()
+    lax.fori_loop(2, 4, hidden_rows(0, 1), 0)
     on_both(2)
-    lax.fori_loop(1, 3, hidden_rows(0), 0)
     on_both(3)
-    lax.fori_loop(3, 4, hidden_rows(0), 0)
     g_dn.on_zh(0)
     for k in range(4):
         for dx in (0, 1):
             res_wait(1, column_of(dx, 1), k)
-    lax.fori_loop(0, 4, hidden_rows(1), 0)
-    g_dn.on_zh(1)
+    lax.fori_loop(0, 4, hidden_rows(1, 0, 1), 0)
 
     mail.settle(passed)
+
+    def mine(group):
+        return (p.c + p.zl + group) % 2 == 0
+
+    def unit(dy, dz, k):
+        return dy * 4 + dz * 2 + k
 
     def sum_own(u, dx):
         return tokens.at[pl.ds((u % 2) * tall, tall), pl.ds((u // 2 * 2 + dx) * block, block)]
 
-    def unit(dy, dz, k):
-        return dy * 4 + dz * 2 + k
-
     def pair(u, dx):
         return sum_own(u, dx)[...].astype(jnp.float32) + sum_cr[u, dx].astype(jnp.float32)
 
-    def x_send_at(n):
-        mail.send(sum_xs.at[n], sum_xr.at[n], x_send.at[n], x_recv.at[n], p.to_x)
-
-    def z_send_at(n):
-        mail.send(sum_zs.at[n], sum_zr.at[n], z_send.at[n], z_recv.at[n], p.to_zl)
-
-    def stage_core(dy, dz, k):
+    def out_part(dy, k):
+        return pl.ds(k * tall, tall), lanes((p.y + dy) % 2 * block, block)
+
+    c_copies = [
+        mail.make(sum_cs.at[u], sum_cr.at[u], c_send.at[u], c_recv.at[u], p.to_c) for u in range(8)
+    ]
+    x_copies = [
+        mail.make(sum_xs.at[n], sum_xr.at[n], x_send.at[n], x_recv.at[n], p.to_x) for n in range(6)
+    ]
+    z_copies = [
+        mail.make(sum_zs.at[n], sum_zr.at[n], z_send.at[n], z_recv.at[n], p.to_zl) for n in range(6)
+    ]
+    mail.started += c_copies + x_copies + z_copies
+    results = [
+        pltpu.make_async_copy(
+            done.at[out_part(n // 2, n % 2)], out.at[out_part(n // 2, n % 2)], local_sem.at[n]
+        )
+        for n in range(4)
+    ]
+
+    def stage_core(group, dy, dz, k):
         u = unit(dy, dz, k)
-        part = hid[(p.zl + dz) % 2, pl.ds(k * tall, tall), :]
-        for dc in (1, 0):
+
+        def term(dx):
+            j = (((p.x + dx) % 2) * 2 + (p.zl + group) % 2) * 2 + (p.y + dy) % 2
+            part = hid[(p.zl + dz) % 2, pl.ds(k * tall, tall), :]
+            value = jnp.dot(part, dn_all[j], preferred_element_type=jnp.float32)
+            return value.astype(jnp.bfloat16)
+
+        @pl.when(mine(group))
+        def _():
             for dx in (0, 1):
-                j = column_of(dx, dc) * 2 + (p.y + dy) % 2
-                term = jnp.dot(part, dn_all[j], preferred_element_type=jnp.float32)
-                if dc == 0:
-                    sum_own(u, dx)[...] = term.astype(jnp.bfloat16)
-                else:
-                    sum_cs[u, dx] = term.astype(jnp.bfloat16)
-            if dc:
-                mail.send(sum_cs.at[u], sum_cr.at[u], c_send.at[u], c_recv.at[u], p.to_c)
-
-    def stage_first(dy, dz, k):
+                sum_own(u, dx)[...] = term(dx)
+
+        @pl.when(mine(1 - group))
+        def _():
+            for dx in (0, 1):
+                sum_cs[u, dx] = term(dx)
+            c_copies[u].start()
+
+    def stage_first(group, dy, dz, k):
         u = unit(dy, dz, k)
-        mail.arrived(sum_cr.at[u], c_recv.at[u])
-        if k == 0:
-            n = dy * 3 + dz
-            sum_xs[n] = pair(u, 1).astype(jnp.bfloat16)
-            x_send_at(n)
-        elif dz == 1:
-            for dx in (1, 0):
-                n = dy * 3 + dx
-                sum_zs[n] = pair(u, dx).astype(jnp.bfloat16)
-                z_send_at(n)
-
-    def stage_second(dy):
+
+        @pl.when(mine(group))
+        def _():
+            mail.arrived(sum_cr.at[u], c_recv.at[u])
+            if k == 0:
+                n = dy * 3 + dz
+                sum_xs[n] = pair(u, 1).astype(jnp.bfloat16)
+                x_copies[n].start()
+            elif dz == 1:
+                for dx in (1, 0):
+                    n = dy * 3 + dx
+                    sum_zs[n] = pair(u, dx).astype(jnp.bfloat16)
+                    z_copies[n].start()
+
+    def from_x(group, dy):
         n = dy * 3
-        mail.arrived(sum_xr.at[n + 1], x_recv.at[n + 1])
-        total = pair(unit(dy, 1, 0), 0) + sum_xr[n + 1].astype(jnp.float32)
-        sum_zs[n + 2] = total.astype(jnp.bfloat16)
-        z_send_at(n + 2)
-        mail.arrived(sum_zr.at[n + 1], z_recv.at[n + 1])
-        total = pair(unit(dy, 0, 1), 1) + sum_zr[n + 1].astype(jnp.float32)
-        sum_xs[n + 2] = total.astype(jnp.bfloat16)
-        x_send_at(n + 2)
-
-    results = []
-
-    def stage_last(dy):
+
+        @pl.when(mine(group))
+        def _():
+            mail.arrived(sum_xr.at[n + 1], x_recv.at[n + 1])
+            total = pair(unit(dy, 1, 0), 0) + sum_xr[n + 1].astype(jnp.float32)
+            sum_zs[n + 2] = total.astype(jnp.bfloat16)
+            z_copies[n + 2].start()
+
+    def from_z(group, dy):
         n = dy * 3
-        side = (p.y + dy) % 2 * block
+
+        @pl.when(mine(group))
+        def _():
+            mail.arrived(sum_zr.at[n + 1], z_recv.at[n + 1])
+            total = pair(unit(dy, 0, 1), 1) + sum_zr[n + 1].astype(jnp.float32)
+            sum_xs[n + 2] = total.astype(jnp.bfloat16)
+            x_copies[n + 2].start()
+
+    def stage_last(dy, k):
+        n = dy * 3
+        first, second = (n, n + 2) if k == 0 else (n + 2, n)
+        mail.arrived(sum_xr.at[first], x_recv.at[first])
+        mail.arrived(sum_zr.at[second], z_recv.at[second])
+        total = pair(unit(dy, 0, k), 0)
+        total = total + sum_xr[first].astype(jnp.float32) + sum_zr[second].astype(jnp.float32)
+        at = pl.ds(k * tall, tall)
+        side = p.column * cols + (p.y + dy) % 2 * block
+        total = total + res[p.zl, at, lanes(side, block)].astype(jnp.float32)
+        done[out_part(dy, k)] = total.astype(jnp.bfloat16)
+        results[dy * 2 + k].start()
+
+    order = [(1, 0), (0, 0), (1, 1), (0, 1)]
+
+    def stage_all(group, dy):
+        for n, (dz, k) in enumerate(order):
+            stage_core(group, dy, dz, k)
+            if n > 1:
+                stage_first(group, dy, *order[n - 2])
+        for n in (2, 3):
+            stage_first(group, dy, *order[n])
+
+    stage_all(0, 0)
+    g_dn.on_zh(1)
+    g_dn.rows_y((0,))
+    stage_all(0, 1)
+    stage_all(1, 0)
+    from_x(0, 0)
+    g_dn.rows_y((1,))
+    stage_all(1, 1)
+    from_z(0, 0)
+    from_x(0, 1)
+    from_z(0, 1)
+    for dy in (0, 1):
+        from_x(1, dy)
+        from_z(1, dy)
+    for dy in (0, 1):
         for k in (0, 1):
-            first, second = (n, n + 2) if k == 0 else (n + 2, n)
-            mail.arrived(sum_xr.at[first], x_recv.at[first])
-            mail.arrived(sum_zr.at[second], z_recv.at[second])
-            total = pair(unit(dy, 0, k), 0)
-            total = total + sum_xr[first].astype(jnp.float32) + sum_zr[second].astype(jnp.float32)
-            at = pl.ds(k * tall, tall)
-            total = total + res[p.zl, at, lanes(p.column * cols + side, block)].astype(jnp.float32)
-            here = (at, lanes(side, block))
-            done[here] = total.astype(jnp.bfloat16)
-            copy = pltpu.make_async_copy(done.at[here], out.at[here], local_sem.at[dy * 2 + k])
-            copy.start()
-            results.append(copy)
-
-    order = [(1, 0), (1, 1), (0, 0), (0, 1)]
-    for dy in (0, 1):
-        if dy:
-            g_dn.rows_y()
-        for n, (dz, k) in enumerate(order):
-            stage_core(dy, dz, k)
-            if n > 1:
-                stage_first(dy, *order[n - 2])
-        for n in (2, 3):
-            stage_first(dy, *order[n])
-    for dy in (0, 1):
-        stage_second(dy)
-    for dy in (0, 1):
-        stage_last(dy)
+            stage_last(dy, k)
     mail.close()
     for copy in results:
         copy.wait()

time: 177 us -> 171 us (0.966)
  Pallas kernels: 173 us -> 167 us
    pallas_call x1, Pallas kernels: 173 us -> 167 us  [local(): pl.pallas_call(fused, out_shape=jax.ShapeDtypeStruct((rows, cols), low_ty...]
where the time goes in v3:
time: 171 us; the launch traced here: 170 us
  Pallas kernels  167 us (98%)
  local copies, waits for them, and re-layouts  2.26 us (1%)
    pallas_call x1, Pallas kernels, local(): pl.pallas_call(fused, out_shape=jax.ShapeDtypeStruct((rows, cols), low_ty...  167 us

profile of v3, /device:TPU:22, one launch (start us, length us, event | category | flops | bytes accessed | tf_op | source)
XLA Modules:
  0.0 169.7 jit_solution(18373670488743586415)
XLA Ops:
  0.0 167.4 %shard_map.127 = bf16[1024,512]{1,0:T(8,128)(2,1)} custom-call(bf16[1024,512]{1,0:T(8,128)(2,1)} %tok.1, f32[256,256]{1,0:T(8,128)} %w_in.1, f32[256,256]{1,0:T(8,128)} %w_out.1, f32[256,1536]{1,0:T(8,128)} %w_gate.1, f32[256,1536]{1,0:T(8,128)} %w_up.1, f32[1536,256]{1,0:T(8,128)} %w_down.1, f32[2048]{0:T(1024)} %gain_mix.1, f32[2048]{0:T(1024)} %gain_ffn.1, ...), custom_call_target="tpu_custom_call" | custom-call | tf_op jit(solution)/shard_map/pallas_call | solution.py:772
  167.4 2.3 %copy.15 = bf16[1024,512]{1,0:T(8,128)(2,1)} copy(bf16[1024,512]{1,0:T(8,128)(2,1)} %shard_map.127) | data formatting | bytes 2097152
